TPU v7x, 32 devices: a whole 2x2x4 slice. The times are simulated.
32 devices in a mesh: sp: 16 (over z, x, core), tp: 2 (over y).
Axes of the slice: x: 2, y: 2, z: 4, core: 2. Of those that a mesh axis runs over, the one named last changes fastest.
Arguments:
- queries: bfloat16 [10240, 1024], P('sp', 'tp'), may hold values from -160 to 160
- keys: bfloat16 [10240, 256], P('sp', 'tp'), may hold values from -24 to 24
- values: bfloat16 [10240, 256], P('sp', 'tp'), may hold values from -6 to 6
- documents: int32 [10240], P('sp'), may hold values from 0 to 3, never falling along the last dimension, each value on 1 to 5120 neighbouring positions
- sinks: float32 [16], P('tp'), may hold values from -1 to 4
- out_weight: bfloat16 [1024, 2048], replicated, may hold values from -0.1875 to 0.1875
- residual: bfloat16 [10240, 2048], P(('sp', 'tp')), may hold values from -3 to 3
- norm_gain: float32 [2048], replicated, may hold values from 0.1 to 1.9
- up_weight: bfloat16 [2048, 8192], P('sp', 'tp'), may hold values from -0.125 to 0.125
- down_weight: bfloat16 [8192, 2048], P('tp', 'sp'), may hold values from -0.0625 to 0.0625
Outputs:
- layer_out: bfloat16 [10240, 2048], P(('sp', 'tp'))
Inputs may be any that keep to these rules, and one draw needn't show every extreme that they name: `documents`: document numbers never fall along the positions; each document holds at most 5120 positions.
All inputs are finite; a program needn't handle non-finite values.
Results may differ from a plain program's by a relative error of at most 0.0095.
Values may be sent and summed in bfloat16 or wider, within the bound.
No kernel may reach another device: no remote copies, remote signals or barrier semaphores. Data moves between devices by JAX's collectives and lax.ppermute only.
A program may use at most 128 MiB of HBM per device.

v0:
```python
import jax
import jax.numpy as jnp
from jax import lax
from jax.sharding import PartitionSpec as P

HEAD_SIZE = 64
WINDOW_REACH = 128


masked_score = -1e30
epsilon = 1e-06


def passed_along(shard, axis, by):
    peers = lax.axis_size(axis)
    pairs = [(i, i + by) for i in range(peers) if 0 <= i + by < peers]
    return lax.ppermute(shard, axis, pairs)


def rounded(value):
    return lax.optimization_barrier(value.astype(jnp.bfloat16))


def squared_relu(before):
    return jnp.square(jax.nn.relu(before)).astype(jnp.bfloat16)


def windowed_attention(queries, keys, values, documents, sinks):
    length = queries.shape[0]
    heads = queries.shape[1] // HEAD_SIZE
    kv_heads = keys.shape[1] // HEAD_SIZE
    query_group = heads // kv_heads
    block_list = length // WINDOW_REACH
    prev_keys, prev_values, prev_docs = passed_along(
        (
            keys[length - WINDOW_REACH :],
            values[length - WINDOW_REACH :],
            documents[length - WINDOW_REACH :],
        ),
        "sp",
        1,
    )
    offset = lax.axis_index("sp") * length
    key_matrix = jnp.concatenate([prev_keys, keys], axis=0).reshape(
        block_list + 1, WINDOW_REACH, kv_heads, HEAD_SIZE
    )
    value_matrix = jnp.concatenate([prev_values, values], axis=0).reshape(
        block_list + 1, WINDOW_REACH, kv_heads, HEAD_SIZE
    )
    key_docs = jnp.concatenate([prev_docs, documents], axis=0).reshape(block_list + 1, WINDOW_REACH)
    key_place = (
        offset - WINDOW_REACH + jnp.arange((block_list + 1) * WINDOW_REACH, dtype=jnp.int32)
    ).reshape(block_list + 1, WINDOW_REACH)
    band_keys = jnp.concatenate([key_matrix[:-1], key_matrix[1:]], axis=1)
    band_values = jnp.concatenate([value_matrix[:-1], value_matrix[1:]], axis=1)
    band_docs = jnp.concatenate([key_docs[:-1], key_docs[1:]], axis=1)
    band_place = jnp.concatenate([key_place[:-1], key_place[1:]], axis=1)
    query_docs = documents.reshape(block_list, WINDOW_REACH)
    grouped_queries = queries.reshape(block_list, WINDOW_REACH, kv_heads, query_group, HEAD_SIZE)
    scores = jnp.einsum(
        "nqhgd,nshd->nhgqs", grouped_queries, band_keys, preferred_element_type=jnp.float32
    ) * HEAD_SIZE ** (-0.5)
    row_index = jnp.arange(WINDOW_REACH, dtype=jnp.int32)[:, None]
    col_index = jnp.arange(2 * WINDOW_REACH, dtype=jnp.int32)[None, :]
    distance = WINDOW_REACH + row_index - col_index
    near = (distance >= 0) & (distance < WINDOW_REACH)
    visible = (
        near[None]
        & (band_docs[:, None, :] == query_docs[:, :, None])
        & (band_place[:, None, :] >= 0)
    )
    visible = visible[:, None, None]
    head_sink_logit = sinks.reshape(kv_heads, query_group)[None, :, :, None]
    scores = jnp.where(visible, scores, masked_score)
    top = jnp.maximum(jnp.max(scores, axis=-1), head_sink_logit)
    exponent = jnp.where(visible, jnp.exp(scores - top[..., None]), 0.0)
    total = jnp.exp(head_sink_logit - top) + jnp.sum(exponent, axis=-1)
    shares = (exponent / total[..., None]).astype(jnp.bfloat16)
    attended = jnp.einsum(
        "nhgqs,nshd->nqhgd", shares, band_values, preferred_element_type=jnp.float32
    )
    return attended.astype(jnp.bfloat16).reshape(length, heads * HEAD_SIZE)


def body(
    queries, keys, values, documents, sinks, out_weight, residual, norm_gain, up_weight, down_weight
):
    up_whole, down_whole = (
        lax.all_gather(up_weight, "sp", axis=0, tiled=True),
        lax.all_gather(down_weight, "sp", axis=1, tiled=True),
    )
    attended = windowed_attention(queries, keys, values, documents, sinks)
    token_heads = lax.all_to_all(attended, "tp", split_axis=0, concat_axis=1, tiled=True)
    projected = jnp.dot(token_heads, out_weight, preferred_element_type=jnp.float32)
    mixed = rounded(residual.astype(jnp.float32) + rounded(projected).astype(jnp.float32))
    widened = mixed.astype(jnp.float32)
    normed = (
        widened
        * lax.rsqrt(jnp.mean(widened * widened, axis=-1, keepdims=True) + epsilon)
        * norm_gain
    ).astype(jnp.bfloat16)
    hidden = squared_relu(
        jnp.dot(
            lax.all_gather(normed, "tp", axis=0, tiled=True),
            up_whole,
            preferred_element_type=jnp.float32,
        )
    )
    branch = lax.psum_scatter(
        jnp.dot(hidden, down_whole, preferred_element_type=jnp.float32).astype(jnp.bfloat16),
        "tp",
        scatter_dimension=0,
        tiled=True,
    ).astype(jnp.float32)
    return (widened + rounded(branch).astype(jnp.float32)).astype(jnp.bfloat16)


def solution(mesh):
    in_specs = (
        P("sp", "tp"),
        P("sp", "tp"),
        P("sp", "tp"),
        P("sp"),
        P("tp"),
        P(),
        P(("sp", "tp"), None),
        P(),
        P("sp", "tp"),
        P("tp", "sp"),
    )
    out_specs = P(("sp", "tp"), None)
    return jax.shard_map(body, mesh=mesh, in_specs=in_specs, out_specs=out_specs, check_vma=False)
```

profile of v0, /device:TPU:0, one launch (start us, length us, event | category | flops | bytes accessed | tf_op | source)
XLA Modules:
  0.0 433.5 jit_solution(7204909823824404609)
XLA Ops:
  6.5 0.8 slice.63
  7.3 2.4 collective-permute-start.1
  9.7 0.8 slice.69
  10.5 4.5 %collective-permute-start.2 = (bf16[128,128]{1,0:T(8,128)(2,1)S(1)}, bf16[128,128]{1,0:T(8,128)(2,1)S(1)}, u32[]{:S(2)}, u32[]{:S(2)}) collective-permute-start(bf16[128,128]{1,0:T(8,128)(2,1)S(1)} %slice.69), channel_id=1, source_target_pairs={{0,2},{2,4},{4,6},{6,8},{8,10},{10,12},{12,14},{14,16},{16,18},{18... | collective-permute-start | bytes 98312 | tf_op jit(solution)/shard_map/ppermute | solution.py:17
  15.0 0.8 slice.59
  15.7 1.9 collective-permute-start
  17.7 1.1 reshape.108
  18.8 1.1 reshape.106
  19.9 2.5 reshape.109
  22.6 0.7 max.25
  23.5 0.7 pad_add_fusion.1
  24.2 0.7 pad_add_fusion
  24.9 0.5 and_and_fusion
  25.8 1.1 fusion
  27.0 2.2 copy-done
  29.2 1.4 fusion.1
  31.1 4.1 fusion.10
  35.2 1.6 copy.53
  36.8 0.8 reshape.110
  37.6 12.8 %all_to_all.19 = bf16[2,320,512]{2,1,0:T(8,128)(2,1)S(1)} all-to-all(bf16[2,320,512]{2,1,0:T(8,128)(2,1)S(1)} %reshape.110), channel_id=1, replica_groups=mesh['sp'=16,'tp'=2] {'tp'}, dimensions={0} | all-to-all | bytes 1310720 | tf_op jit(solution)/shard_map/all_to_all | solution.py:93
  50.5 3.8 convolution_convert_fusion.1
  54.4 0.5 add_convert_fusion
  54.8 0.4 fusion.2
  55.2 1.4 fusion.4
  56.7 0.7 all-gather.6.cloned.1.call-update
  57.5 0.7 all-gather.8.cloned.1.call-update
  58.4 36.8 %all-gather.4.cloned.1.call-done = bf16[640,2048]{1,0:T(8,128)(2,1)} async-done(((bf16[320,2048]{1,0:T(8,128)(2,1)}), bf16[640,2048]{1,0:T(8,128)(2,1)}) %all-gather.4.cloned.1.call-update) | async-done | bytes 2621456 | tf_op jit(solution)/shard_map/all_gather | solution.py:104
  95.2 128.6 %all-gather.6.cloned.1.call-done = bf16[2048,4096]{1,0:T(8,128)(2,1)} async-done(((bf16[128,4096]{1,0:T(8,128)(2,1)}), bf16[2048,4096]{1,0:T(8,128)(2,1)}) %all-gather.6.cloned.1.call-update) | async-done | bytes 16777232 | tf_op jit(solution)/shard_map/all_gather | solution.py:89
  223.8 130.3 %all-gather.8.cloned.1.call-done = bf16[4096,2048]{1,0:T(8,128)(2,1)} async-done(((bf16[4096,128]{1,0:T(8,128)(2,1)}), bf16[4096,2048]{1,0:T(8,128)(2,1)}) %all-gather.8.cloned.1.call-update) | async-done | bytes 16777232 | tf_op jit(solution)/shard_map/all_gather | solution.py:90
  354.1 34.0 %convolution_convert_fusion = bf16[640,2048]{1,0:T(8,128)(2,1)} fusion(bf16[4096,2048]{1,0:T(8,128)(2,1)} %all-gather.8.cloned.1.call-done, bf16[640,2048]{1,0:T(8,128)(2,1)} %all-gather.4.cloned.1.call-done, bf16[2048,4096]{1,0:T(8,128)(2,1)} %all-gather.6.cloned.1.call-done), kind=kOutput, calls=%fused_computation.9 | convolution fusion | flops 21484011520 | bytes 38797312 | tf_op jit(solution)/shard_map/dot_general | solution.py:110
  388.1 36.0 %reduce-scatter.2.cloned.1.call-done = bf16[320,2048]{1,0:T(8,128)(2,1)} async-done(((bf16[640,2048]{1,0:T(8,128)(2,1)}), bf16[320,2048]{1,0:T(8,128)(2,1)}) %reduce-scatter.2.cloned.1.call-update) | async-done | bytes 1310736 | tf_op jit(solution)/shard_map/reduce_scatter | solution.py:109
  424.1 2.9 fusion.5
  (38 shorter events, 1.8 us)
Async XLA Ops:
  6.5 18.4 %copy-start.4 = (s32[640]{0:T(1024)S(1)}, s32[640]{0:T(1024)}, u32[]{:S(2)}) copy-start(s32[640]{0:T(1024)} %param.13) | copy-start | bytes 7684
  6.5 18.9 %copy-start.2 = (bf16[640,128]{1,0:T(8,128)(2,1)S(1)}, bf16[640,128]{1,0:T(8,128)(2,1)}, u32[]{:S(2)}) copy-start(bf16[640,128]{1,0:T(8,128)(2,1)} %param.11) | copy-start | bytes 491524
  6.5 88.7 %all-gather.4.cloned.1.call-start = ((), (), s32[]{:S(2)}) async-start(), calls=%async_computation.2 | async-start | bytes 3932160 | tf_op jit(solution)/shard_map/all_gather | solution.py:104
  7.3 16.2 %collective-permute-start.1 = (s32[128]{0:T(128)S(1)}, s32[128]{0:T(128)S(1)}, u32[]{:S(2)}, u32[]{:S(2)}) collective-permute-start(s32[128]{0:T(128)S(1)} %slice.63), channel_id=1, source_target_pairs={{0,2},{2,4},{4,6},{6,8},{8,10},{10,12},{12,14},{14,16},{16,18},{18... | collective-permute-start | bytes 1544 | tf_op jit(solution)/shard_map/ppermute | solution.py:17
  10.5 15.0 %collective-permute-start.2 = (bf16[128,128]{1,0:T(8,128)(2,1)S(1)}, bf16[128,128]{1,0:T(8,128)(2,1)S(1)}, u32[]{:S(2)}, u32[]{:S(2)}) collective-permute-start(bf16[128,128]{1,0:T(8,128)(2,1)S(1)} %slice.69), channel_id=1, source_target_pairs={{0,2},{2,4},{4,6},{6,8},{8,10},{10,12},{12,14},{14,16},{16,18},{18... | collective-permute-start | bytes 98312 | tf_op jit(solution)/shard_map/ppermute | solution.py:17
  15.7 15.0 %collective-permute-start = (bf16[128,128]{1,0:T(8,128)(2,1)S(1)}, bf16[128,128]{1,0:T(8,128)(2,1)S(1)}, u32[]{:S(2)}, u32[]{:S(2)}) collective-permute-start(bf16[128,128]{1,0:T(8,128)(2,1)S(1)} %slice.59), channel_id=1, source_target_pairs={{0,2},{2,4},{4,6},{6,8},{8,10},{10,12},{12,14},{14,16},{16,18},{18... | collective-permute-start | bytes 98312 | tf_op jit(solution)/shard_map/ppermute | solution.py:17
  26.9 2.3 copy-start
  26.9 3.8 copy-start.3
  50.5 3.8 copy-start.1
  54.4 0.9 copy-start.5
  56.7 167.2 %all-gather.6.cloned.1.call-start = ((), (), s32[]{:S(2)}) async-start(), calls=%async_computation.3 | async-start | bytes 17825792 | tf_op jit(solution)/shard_map/all_gather | solution.py:89
  57.4 296.7 %all-gather.8.cloned.1.call-start = ((), (), s32[]{:S(2)}) async-start(), calls=%async_computation.4 | async-start | bytes 17825792 | tf_op jit(solution)/shard_map/all_gather | solution.py:90
  58.2 366.0 %reduce-scatter.2.cloned.1.call-start = ((), (), s32[]{:S(2)}) async-start(), calls=%async_computation.5 | async-start | bytes 3932160 | tf_op jit(solution)/shard_map/reduce_scatter | solution.py:109
Sparse Core Ops, SparseCore 0:
  56.8 38.3 all-gather.3
  97.4 126.4 all-gather.5
  226.0 128.0 all-gather.7
  388.2 35.8 reduce-scatter.1
where the time goes:
time: 434 us
  waiting for transfers between devices  333 us (77%)
  matrix products  42.9 us (10%)
  local copies, waits for them, and re-layouts  13.4 us (3%)
  between operations  13.4 us (3%)
  blocking collectives  12.8 us (3%)
  starting transfers between devices  9.08 us (2%)
  other arithmetic  8.68 us (2%)
    all_gather x1, waiting for transfers between devices, body(): lax.all_gather(down_weight, 'sp', axis=1, tiled=True)  130 us
    all_gather x1, waiting for transfers between devices, body(): lax.all_gather(up_weight, 'sp', axis=0, tiled=True)  129 us
    all_gather x1, waiting for transfers between devices, body(): lax.all_gather(normed, 'tp', axis=0, tiled=True)  36.8 us
    reduce_scatter x1, waiting for transfers between devices, body(): lax.psum_scatter(jnp.dot(hidden, down_whole, preferred_element_type=jnp.f...  36 us
    dot_general x1, matrix products, body(): jnp.dot(hidden, down_whole, preferred_element_type=jnp.float32)  34 us
    all_to_all x1, blocking collectives, body(): lax.all_to_all(attended, 'tp', split_axis=0, concat_axis=1, tiled=True)  12.8 us
    ppermute x3, starting transfers between devices, passed_along(): return lax.ppermute(shard, axis, pairs)  8.78 us
  transfers between devices with their start and end apart: 7, of which 4 were waited for; matrix products, arithmetic and copies ran while one was open for 3% of the time, Pallas kernels for 0%

commit v1 on v0

--- a/solution.py
+++ b/solution.py
@@ -15,6 +15,11 @@
     peers = lax.axis_size(axis)
     pairs = [(i, i + by) for i in range(peers) if 0 <= i + by < peers]
     return lax.ppermute(shard, axis, pairs)
+
+
+def turned(shard, axis, by):
+    peers = lax.axis_size(axis)
+    return lax.ppermute(shard, axis, [(i, (i + by) % peers) for i in range(peers)])
 
 
 def rounded(value):
@@ -82,13 +87,36 @@
     return attended.astype(jnp.bfloat16).reshape(length, heads * HEAD_SIZE)
 
 
+def gathered_rows(rows, axis):
+    peers = lax.axis_size(axis)
+    place = lax.axis_index(axis)
+    count = rows.shape[0]
+    whole = jnp.zeros((peers * count, rows.shape[1]), rows.dtype)
+    for by in range(peers):
+        piece = turned(rows, axis, by) if by else rows
+        whole = lax.dynamic_update_slice(whole, piece, (((place - by) % peers) * count, 0))
+    return whole
+
+
+def scattered_sum(partial, axis):
+    peers = lax.axis_size(axis)
+    place = lax.axis_index(axis)
+    count = partial.shape[0] // peers
+    total = None
+    for by in range(peers):
+        piece = lax.dynamic_slice(
+            partial, (((place + by) % peers) * count, 0), (count, partial.shape[1])
+        )
+        piece = (turned(piece, axis, by) if by else piece).astype(jnp.float32)
+        total = piece if total is None else total + piece
+    return total
+
+
 def body(
     queries, keys, values, documents, sinks, out_weight, residual, norm_gain, up_weight, down_weight
 ):
-    up_whole, down_whole = (
-        lax.all_gather(up_weight, "sp", axis=0, tiled=True),
-        lax.all_gather(down_weight, "sp", axis=1, tiled=True),
-    )
+    up_whole = lax.all_gather(up_weight, "sp", axis=0, tiled=True)
+    down_whole = lax.all_gather(down_weight, "sp", axis=1, tiled=True)
     attended = windowed_attention(queries, keys, values, documents, sinks)
     token_heads = lax.all_to_all(attended, "tp", split_axis=0, concat_axis=1, tiled=True)
     projected = jnp.dot(token_heads, out_weight, preferred_element_type=jnp.float32)
@@ -100,18 +128,10 @@
         * norm_gain
     ).astype(jnp.bfloat16)
     hidden = squared_relu(
-        jnp.dot(
-            lax.all_gather(normed, "tp", axis=0, tiled=True),
-            up_whole,
-            preferred_element_type=jnp.float32,
-        )
+        jnp.dot(gathered_rows(normed, "tp"), up_whole, preferred_element_type=jnp.float32)
     )
-    branch = lax.psum_scatter(
-        jnp.dot(hidden, down_whole, preferred_element_type=jnp.float32).astype(jnp.bfloat16),
-        "tp",
-        scatter_dimension=0,
-        tiled=True,
-    ).astype(jnp.float32)
+    partial = jnp.dot(hidden, down_whole, preferred_element_type=jnp.float32).astype(jnp.bfloat16)
+    branch = scattered_sum(partial, "tp")
     return (widened + rounded(branch).astype(jnp.float32)).astype(jnp.bfloat16)
 
 

time: 434 us -> 345 us (0.79)
  waiting for transfers between devices: 333 us -> 256 us
  blocking collectives: 12.8 us -> 0 us
  starting transfers between devices: 9.08 us -> 14.1 us
    all_gather x3 -> x2, waiting for transfers between devices: 296 us -> 183 us  [the longest x1 130 us: body(): down_whole = lax.all_gather(down_weight, 'sp', axis=1, tiled=True)]
    ppermute x0 -> x2, waiting for transfers between devices: none -> 61.3 us  [turned(): lax.ppermute(shard, axis, [(i, (i + by) % peers) for i in range(peers)])]
    reduce_scatter x1 -> x0, waiting for transfers between devices: 36 us -> none  [body(): lax.psum_scatter(jnp.dot(hidden, down_whole, preferred_element_type=jnp.f...]
    all_to_all x1 -> x0, blocking collectives: 12.8 us -> none  [body(): lax.all_to_all(attended, 'tp', split_axis=0, concat_axis=1, tiled=True)]
    all_to_all x0 -> x1, waiting for transfers between devices: none -> 9.9 us  [body(): lax.all_to_all(attended, 'tp', split_axis=0, concat_axis=1, tiled=True)]
  transfers between devices with their start and end apart: 7 -> 8, of which waited for: 4 -> 5; matrix products, arithmetic and copies ran while one was open for 3% -> 7% of each run, Pallas kernels for 0% -> 0%
where the time goes in v1:
time: 345 us; the launch traced here: 344 us
  waiting for transfers between devices  256 us (74%)
  matrix products  40.4 us (12%)
  starting transfers between devices  14.1 us (4%)
  between operations  13.8 us (4%)
  local copies, waits for them, and re-layouts  13.3 us (4%)
  other arithmetic  7.01 us (2%)
    all_gather x1, waiting for transfers between devices, body(): down_whole = lax.all_gather(down_weight, 'sp', axis=1, tiled=True)  130 us
    ppermute x2, waiting for transfers between devices, turned(): lax.ppermute(shard, axis, [(i, (i + by) % peers) for i in range(peers)])  61.3 us
    all_gather x1, waiting for transfers between devices, body(): up_whole = lax.all_gather(up_weight, 'sp', axis=0, tiled=True)  53.1 us
    dot_general x1, matrix products, body(): jnp.dot(hidden, down_whole, preferred_element_type=jnp.float32)  34 us
    all_to_all x1, waiting for transfers between devices, body(): lax.all_to_all(attended, 'tp', split_axis=0, concat_axis=1, tiled=True)  9.9 us
    ppermute x3, starting transfers between devices, passed_along(): return lax.ppermute(shard, axis, pairs)  8.78 us
  transfers between devices with their start and end apart: 8, of which 5 were waited for; matrix products, arithmetic and copies ran while one was open for 7% of the time, Pallas kernels for 0%

profile of v1, /device:TPU:0, one launch (start us, length us, event | category | flops | bytes accessed | tf_op | source)
XLA Modules:
  0.0 344.4 jit_solution(5409566155315537250)
XLA Ops:
  6.5 0.7 all-gather.3.cloned.1.call-update
  7.3 0.7 all-gather.5.cloned.1.call-update
  8.0 0.7 slice.63
  8.7 2.4 collective-permute-start.1
  11.1 0.8 slice.69
  11.9 4.5 %collective-permute-start.2 = (bf16[128,128]{1,0:T(8,128)(2,1)S(1)}, bf16[128,128]{1,0:T(8,128)(2,1)S(1)}, u32[]{:S(2)}, u32[]{:S(2)}) collective-permute-start(bf16[128,128]{1,0:T(8,128)(2,1)S(1)} %slice.69), channel_id=1, source_target_pairs={{0,2},{2,4},{4,6},{6,8},{8,10},{10,12},{12,14},{14,16},{16,18},{18... | collective-permute-start | bytes 98312 | tf_op jit(solution)/shard_map/ppermute | solution.py:17
  16.4 0.8 slice.59
  17.1 1.9 collective-permute-start
  19.2 1.1 reshape.108
  20.5 0.7 reshape.109
  21.7 0.5 and_and_fusion
  23.0 1.1 fusion
  24.1 1.4 fusion.1
  25.7 1.6 fusion.10
  27.2 1.6 copy.53
  28.9 1.6 reshape.110
  30.5 3.7 %all-to-all-start = ((bf16[2,320,512]{2,1,0:T(8,128)(2,1)}), bf16[2,320,512]{2,1,0:T(8,128)(2,1)S(1)}, u32[]{:S(2)}, u32[]{:S(2)}) async-start(bf16[2,320,512]{2,1,0:T(8,128)(2,1)} %reshape.110), calls=%async_computation | async-start | bytes 1310720 | tf_op jit(solution)/shard_map/all_to_all | solution.py:121
  34.2 9.9 %all-to-all-done = bf16[2,320,512]{2,1,0:T(8,128)(2,1)S(1)} async-done(((bf16[2,320,512]{2,1,0:T(8,128)(2,1)}), bf16[2,320,512]{2,1,0:T(8,128)(2,1)S(1)}, u32[]{:S(2)}, u32[]{:S(2)}) %all-to-all-start) | async-done | bytes 655392 | tf_op jit(solution)/shard_map/all_to_all | solution.py:121
  44.2 3.8 %convolution_convert_fusion.1 = bf16[320,2048]{1,0:T(8,128)(2,1)S(1)} fusion(bf16[320,1024]{1,0:T(8,128)(2,1)S(1)} %bitcast.50, bf16[1024,2048]{1,0:T(8,128)(2,1)} %param.15), kind=kOutput, calls=%fused_computation.10 | convolution fusion | flops 1342832640 | bytes 6160384 | tf_op jit(solution)/shard_map/dot_general | solution.py:122
  48.0 0.5 add_convert_fusion.1
  48.9 1.9 broadcast_in_dim.34
  50.7 1.9 constant_dynamic-update-slice_fusion.1
  52.6 31.8 %collective-permute-done.3 = bf16[320,2048]{1,0:T(8,128)(2,1)S(1)} collective-permute-done((bf16[320,2048]{1,0:T(8,128)(2,1)}, bf16[320,2048]{1,0:T(8,128)(2,1)S(1)}, u32[]{:S(2)}, u32[]{:S(2)}) %collective-permute-start.3) | collective-permute-done | bytes 1310752 | tf_op jit(solution)/shard_map/ppermute | solution.py:22
  84.4 1.2 constant_dynamic-update-slice_fusion
  85.6 53.1 %all-gather.3.cloned.1.call-done = bf16[2048,4096]{1,0:T(8,128)(2,1)} async-done(((bf16[128,4096]{1,0:T(8,128)(2,1)}), bf16[2048,4096]{1,0:T(8,128)(2,1)}) %all-gather.3.cloned.1.call-update) | async-done | bytes 16777232 | tf_op jit(solution)/shard_map/all_gather | solution.py:118
  138.7 130.2 %all-gather.5.cloned.1.call-done = bf16[4096,2048]{1,0:T(8,128)(2,1)} async-done(((bf16[4096,128]{1,0:T(8,128)(2,1)}), bf16[4096,2048]{1,0:T(8,128)(2,1)}) %all-gather.5.cloned.1.call-update) | async-done | bytes 16777232 | tf_op jit(solution)/shard_map/all_gather | solution.py:119
  268.9 34.0 %convolution_convert_fusion = bf16[640,2048]{1,0:T(8,128)(2,1)} fusion(bf16[4096,2048]{1,0:T(8,128)(2,1)} %all-gather.5.cloned.1.call-done, bf16[640,2048]{1,0:T(8,128)(2,1)} %constant_dynamic-update-slice_fusion, bf16[2048,4096]{1,0:T(8,128)(2,1)} %all-gather.3.cloned.1.call-done), kind=kOutput, calls=%fused_computation.9 | convolution fusion | flops 21484011520 | bytes 38797312 | tf_op jit(solution)/shard_map/dot_general | solution.py:133
  302.9 1.6 constant_dynamic-slice_fusion
  304.5 1.6 collective-permute-start.4
  306.1 29.4 %collective-permute-done.4 = bf16[320,2048]{1,0:T(8,128)(2,1)S(1)} collective-permute-done((bf16[320,2048]{1,0:T(8,128)(2,1)S(1)}, bf16[320,2048]{1,0:T(8,128)(2,1)S(1)}, u32[]{:S(2)}, u32[]{:S(2)}) %collective-permute-start.4) | collective-permute-done | bytes 1310752 | tf_op jit(solution)/shard_map/ppermute | solution.py:22
  335.5 0.5 add_convert_fusion
  336.1 1.5 fusion.5
  (45 shorter events, 2.1 us)
Async XLA Ops:
  6.5 13.7 %copy-start.3 = (bf16[640,128]{1,0:T(8,128)(2,1)S(1)}, bf16[640,128]{1,0:T(8,128)(2,1)}, u32[]{:S(2)}) copy-start(bf16[640,128]{1,0:T(8,128)(2,1)} %param.12) | copy-start | bytes 491524
  6.5 13.9 %copy-start.4 = (bf16[640,512]{1,0:T(8,128)(2,1)S(1)}, bf16[640,512]{1,0:T(8,128)(2,1)}, u32[]{:S(2)}) copy-start(bf16[640,512]{1,0:T(8,128)(2,1)} %param.10) | copy-start | bytes 1966084
  6.5 14.8 %copy-start.7 = (f32[8]{0:T(128)S(1)}, f32[8]{0:T(128)}, u32[]{:S(2)}) copy-start(f32[8]{0:T(128)} %param.14) | copy-start | bytes 100
  6.5 132.1 %all-gather.3.cloned.1.call-start = ((), (), s32[]{:S(2)}) async-start(), calls=%async_computation.1 | async-start | bytes 17825792 | tf_op jit(solution)/shard_map/all_gather | solution.py:118
  7.3 14.3 %copy-start.5 = (s32[640]{0:T(1024)S(1)}, s32[640]{0:T(1024)}, u32[]{:S(2)}) copy-start(s32[640]{0:T(1024)} %param.13) | copy-start | bytes 7684
  7.3 14.9 %copy-start.2 = (bf16[640,128]{1,0:T(8,128)(2,1)S(1)}, bf16[640,128]{1,0:T(8,128)(2,1)}, u32[]{:S(2)}) copy-start(bf16[640,128]{1,0:T(8,128)(2,1)} %param.11) | copy-start | bytes 491524
  7.3 261.7 %all-gather.5.cloned.1.call-start = ((), (), s32[]{:S(2)}) async-start(), calls=%async_computation.2 | async-start | bytes 17825792 | tf_op jit(solution)/shard_map/all_gather | solution.py:119
  8.7 12.9 %collective-permute-start.1 = (s32[128]{0:T(128)S(1)}, s32[128]{0:T(128)S(1)}, u32[]{:S(2)}, u32[]{:S(2)}) collective-permute-start(s32[128]{0:T(128)S(1)} %slice.63), channel_id=1, source_target_pairs={{0,2},{2,4},{4,6},{6,8},{8,10},{10,12},{12,14},{14,16},{16,18},{18... | collective-permute-start | bytes 1544 | tf_op jit(solution)/shard_map/ppermute | solution.py:17
  11.9 10.3 %collective-permute-start.2 = (bf16[128,128]{1,0:T(8,128)(2,1)S(1)}, bf16[128,128]{1,0:T(8,128)(2,1)S(1)}, u32[]{:S(2)}, u32[]{:S(2)}) collective-permute-start(bf16[128,128]{1,0:T(8,128)(2,1)S(1)} %slice.69), channel_id=1, source_target_pairs={{0,2},{2,4},{4,6},{6,8},{8,10},{10,12},{12,14},{14,16},{16,18},{18... | collective-permute-start | bytes 98312 | tf_op jit(solution)/shard_map/ppermute | solution.py:17
  17.1 5.4 %collective-permute-start = (bf16[128,128]{1,0:T(8,128)(2,1)S(1)}, bf16[128,128]{1,0:T(8,128)(2,1)S(1)}, u32[]{:S(2)}, u32[]{:S(2)}) collective-permute-start(bf16[128,128]{1,0:T(8,128)(2,1)S(1)} %slice.59), channel_id=1, source_target_pairs={{0,2},{2,4},{4,6},{6,8},{8,10},{10,12},{12,14},{14,16},{16,18},{18... | collective-permute-start | bytes 98312 | tf_op jit(solution)/shard_map/ppermute | solution.py:17
  30.5 13.6 %all-to-all-start = ((bf16[2,320,512]{2,1,0:T(8,128)(2,1)}), bf16[2,320,512]{2,1,0:T(8,128)(2,1)S(1)}, u32[]{:S(2)}, u32[]{:S(2)}) async-start(bf16[2,320,512]{2,1,0:T(8,128)(2,1)} %reshape.110), calls=%async_computation | async-start | bytes 1310720 | tf_op jit(solution)/shard_map/all_to_all | solution.py:121
  44.2 3.8 %copy-start.1 = (bf16[320,2048]{1,0:T(8,128)(2,1)S(1)}, bf16[320,2048]{1,0:T(8,128)(2,1)}, u32[]{:S(2)}) copy-start(bf16[320,2048]{1,0:T(8,128)(2,1)} %param.16) | copy-start | bytes 3932164
  48.5 2.2 copy-start.6
  52.6 31.8 %collective-permute-start.3 = (bf16[320,2048]{1,0:T(8,128)(2,1)}, bf16[320,2048]{1,0:T(8,128)(2,1)S(1)}, u32[]{:S(2)}, u32[]{:S(2)}) collective-permute-start(bf16[320,2048]{1,0:T(8,128)(2,1)} %get-tuple-element.6), channel_id=1, source_target_pairs={{0,1},{1,0},{2,3},{3,2},{4,5},{5,4},{6,7},{7,6},{8,9},{9,8},{10,11... | collective-permute-start | bytes 3932168 | tf_op jit(solution)/shard_map/ppermute | solution.py:22
  302.9 32.6 %copy-start = (bf16[640,2048]{1,0:T(8,128)(2,1)S(1)}, bf16[640,2048]{1,0:T(8,128)(2,1)}, u32[]{:S(2)}) copy-start(bf16[640,2048]{1,0:T(8,128)(2,1)} %convolution_convert_fusion) | copy-start | bytes 7864324
  304.5 31.0 %collective-permute-start.4 = (bf16[320,2048]{1,0:T(8,128)(2,1)S(1)}, bf16[320,2048]{1,0:T(8,128)(2,1)S(1)}, u32[]{:S(2)}, u32[]{:S(2)}) collective-permute-start(bf16[320,2048]{1,0:T(8,128)(2,1)S(1)} %constant_dynamic-slice_fusion), channel_id=1, source_target_pairs={{0,1},{1,0},{2,3},{3,2},{4,5},{5,4},{6,7},{7,6},{8,9},{9,8},{10,11... | collective-permute-start | bytes 3932168 | tf_op jit(solution)/shard_map/ppermute | solution.py:22
Sparse Core Ops, SparseCore 0:
  9.5 129.1 all-gather.2
  140.8 128.0 all-gather.4
